TPU v7x, 32 devices: a whole 2x2x4 slice. The times are simulated.
32 devices in a mesh: gr: 2 (over y), sp: 4 (over z), tp: 4 (over x, core).
Axes of the slice: x: 2, y: 2, z: 4, core: 2. Of those that a mesh axis runs over, the one named last changes fastest.
Arguments:
- layer_input: bfloat16 [2, 3072, 2048], P('gr', ('sp', 'tp')), may hold values from -6 to 6
- key_weight: bfloat16 [2048, 2048], P(None, 'tp'), may hold values from -0.125 to 0.125
- value_weight: bfloat16 [2048, 2048], P(None, 'tp'), may hold values from -0.125 to 0.125
- new_queries: bfloat16 [2, 2048], P('gr', 'tp'), may hold values from -280 to 280
- lambdas: float32 [16], P('tp'), may hold values from 0.3 to 0.8
- head_gain: float32 [128], replicated, may hold values from 0.1 to 1.9
- out_weight: bfloat16 [2048, 2048], P('tp'), may hold values from -0.125 to 0.125
Outputs:
- key_cache: bfloat16 [2, 3072, 2048], P('gr', 'sp', 'tp')
- value_cache: bfloat16 [2, 3072, 2048], P('gr', 'sp', 'tp')
- mixed: bfloat16 [2, 2048], P('gr', 'tp')
All inputs are finite; a program needn't handle non-finite values.
Results may differ from a plain program's by a relative error of at most 0.03.
Values may be sent and summed in bfloat16 or wider, within the bound.
No kernel may reach another device: no remote copies, remote signals or barrier semaphores. Data moves between devices by JAX's collectives and lax.ppermute only.
A program may use at most 64 MiB of HBM per device.

v0:
```python
import functools

import jax
import jax.numpy as jnp
from jax import lax
from jax.experimental import pallas as pl
from jax.experimental.pallas import tpu as pltpu
from jax.sharding import PartitionSpec as P


LANES = 128
F32 = jnp.float32
BF16 = jnp.bfloat16


def rope_table(first_position, count, head_dim):
    inverse = 1.0 / 10000.0 ** (jnp.arange(0, head_dim, 2, dtype=F32) / head_dim)
    positions = first_position + jnp.arange(count, dtype=jnp.int32)
    angles = positions.astype(F32)[:, None] * inverse[None, :]
    cosine, sine = jnp.cos(angles), jnp.sin(angles)
    return jnp.concatenate([cosine, cosine, -sine, sine], axis=-1)


def turn(rows, table, head_dim):
    half = head_dim // 2
    lane = lax.broadcasted_iota(jnp.int32, rows.shape, 1)
    swapped = pltpu.roll(table, head_dim, 1)
    low = lane < head_dim
    cosine = jnp.where(low, table, swapped)
    sine = jnp.where(low, swapped, table)
    left = pltpu.roll(rows, LANES - half, 1)
    right = pltpu.roll(rows, half, 1)
    turned = jnp.where(lane % head_dim < half, left, right)
    return rows * cosine + turned * sine


def project_kernel(pieces, heads, head_dim, tile, first, *refs):
    count = len(pieces)
    x_refs, refs = refs[:count], refs[count:]
    wk_ref, wv_ref, q_ref, table_ref, refs = refs[0], refs[1], refs[2], refs[3], refs[4:]
    if not first:
        before_ref, refs = refs[0], refs[3:]
    k_out, v_out, state_ref, xs, kbuf, vbuf, o_sem = refs
    me = lax.axis_index("tp")
    block_rows = pieces[0][3]
    columns = wk_ref.shape[1]
    lengths = [piece[2] for piece in pieces]
    starts = [sum(lengths[:i]) for i in range(count)]
    total = sum(lengths)
    offsets = [
        pl.multiple_of(source(me) * block_rows + row, 16) for source, row, _, _ in pieces
    ]
    if count > 1 and total <= xs.shape[0]:
        for i in range(count):
            xs[pl.ds(starts[i], lengths[i]), :] = x_refs[i][...]
        spans = [(xs, 0, total)]
    else:
        spans = [(x_refs[i], starts[i], lengths[i]) for i in range(count)]
    tables = [table_ref[pl.ds(offsets[i], lengths[i]), :] for i in range(count)]
    table = tables[0] if count == 1 else jnp.concatenate(tables, axis=0)

    def writes(buffer, out, base):
        return [
            pltpu.make_async_copy(
                buffer.at[pl.ds(starts[i], lengths[i])],
                out.at[pl.ds(offsets[i], lengths[i])],
                o_sem.at[base + i],
            )
            for i in range(count)
        ]

    for c in range(0, columns, tile):
        for x_ref, row, length in spans:
            raw = jnp.dot(
                x_ref[...], wk_ref[:, pl.ds(c, tile)], preferred_element_type=F32
            )
            for d in range(0, tile, LANES):
                turned = turn(raw[:, d : d + LANES], table[row : row + length], head_dim)
                kbuf[pl.ds(row, length), pl.ds(c + d, LANES)] = turned.astype(BF16)
    k_writes = writes(kbuf, k_out, 0)
    for copy in k_writes:
        copy.start()
    for c in range(0, columns, tile):
        for x_ref, row, length in spans:
            raw = jnp.dot(
                x_ref[...], wv_ref[:, pl.ds(c, tile)], preferred_element_type=F32
            )
            vbuf[pl.ds(row, length), pl.ds(c, tile)] = raw.astype(BF16)
    v_writes = writes(vbuf, v_out, count)
    for copy in v_writes:
        copy.start()

    lines = state_ref.shape[0] // 3
    line = lax.broadcasted_iota(jnp.int32, (lines, columns), 0)
    lane = lax.broadcasted_iota(jnp.int32, (lines, columns), 1)
    mine = lane // head_dim == (line % heads) * 2 + line // heads
    spread = jnp.broadcast_to(q_ref[...].astype(F32), (lines, columns))
    queries = jnp.where(mine, spread, 0.0).astype(BF16)
    scores = lax.dot_general(
        queries, kbuf[...], (((1,), (1,)), ((), ())), preferred_element_type=F32
    )
    scores = scores * head_dim ** (-0.5)
    highest = jnp.max(scores, axis=1, keepdims=True)
    if not first:
        earlier = before_ref[pl.ds(lines, lines), :][:, :1]
        highest = jnp.maximum(highest, earlier)
    weights = jnp.exp(scores - highest)
    totals = jnp.sum(weights, axis=1, keepdims=True)
    coarse = weights.astype(BF16)
    fine = (weights - coarse.astype(F32)).astype(BF16)
    values = vbuf[...]
    wide = jnp.dot(coarse, values, preferred_element_type=F32)
    wide = wide + jnp.dot(fine, values, preferred_element_type=F32)
    row_id = lax.broadcasted_iota(jnp.int32, (lines, 2 * head_dim), 0)
    weighted = jnp.zeros((lines, 2 * head_dim), F32)
    for h in range(heads):
        part = wide[:, h * 2 * head_dim : (h + 1) * 2 * head_dim]
        weighted = jnp.where(row_id % heads == h, part, weighted)
    if not first:
        factor = jnp.exp(earlier - highest)
        weighted = weighted + before_ref[pl.ds(0, lines), :] * factor
        totals = totals + before_ref[pl.ds(2 * lines, lines), :][:, :1] * factor
    state_ref[pl.ds(0, lines), :] = weighted
    state_ref[pl.ds(lines, lines), :] = jnp.broadcast_to(highest, (lines, 2 * head_dim))
    state_ref[pl.ds(2 * lines, lines), :] = jnp.broadcast_to(totals, (lines, 2 * head_dim))
    for copy in k_writes + v_writes:
        copy.wait()


def project(arrays, pieces, wk, wv, queries, table, heads, head_dim, all_rows, carried):
    depth, columns = wk.shape
    tile = min(256, columns)
    total = sum(piece[2] for piece in pieces)
    lines = max(8, 2 * heads)
    count = len(pieces)
    anywhere = pl.BlockSpec(memory_space=pltpu.HBM)
    vmem = pl.BlockSpec(memory_space=pltpu.VMEM)
    first = carried is None
    operands = [*arrays, wk, wv, queries, table]
    in_specs = [vmem] * (count + 4)
    aliases = {}
    if not first:
        state, keys, values = carried
        operands += [state, keys, values]
        in_specs += [vmem, anywhere, anywhere]
        aliases = {count + 5: 0, count + 6: 1}
    cache = jax.ShapeDtypeStruct((all_rows, columns), BF16)
    keys, values, state = pl.pallas_call(
        functools.partial(project_kernel, pieces, heads, head_dim, tile, first),
        in_specs=in_specs,
        out_specs=[anywhere, anywhere, vmem],
        out_shape=[cache, cache, jax.ShapeDtypeStruct((3 * lines, 2 * head_dim), F32)],
        input_output_aliases=aliases,
        scratch_shapes=[
            pltpu.VMEM((min(total, 256) if count > 1 else 16, depth), BF16),
            pltpu.VMEM((total, columns), BF16),
            pltpu.VMEM((total, columns), BF16),
            pltpu.SemaphoreType.DMA((2 * count,)),
        ],
        compiler_params=pltpu.CompilerParams(vmem_limit_bytes=32 * 1024 * 1024),
        cost_estimate=pl.CostEstimate(
            flops=4 * total * depth * columns,
            transcendentals=0,
            bytes_accessed=4 * depth * columns + 2 * total * (depth + 2 * columns),
        ),
    )(*operands)
    return state, keys, values


def finish_kernel(groups, heads, parts, *refs):
    state_refs = refs[: len(groups)]
    lambda_ref, gain_ref, w_ref = refs[len(groups) : len(groups) + 3]
    outs = refs[len(groups) + 3 : len(groups) + 3 + parts]
    board = refs[-1]
    me = lax.axis_index("tp")
    states = [ref[i] for ref, size in zip(state_refs, groups) for i in range(size)]
    lines = states[0].shape[0] // 3
    highest = functools.reduce(jnp.maximum, [s[lines : 2 * lines] for s in states])
    weighted, totals = 0.0, 0.0
    for s in states:
        factor = jnp.exp(s[lines : 2 * lines] - highest)
        weighted = weighted + s[:lines] * factor
        totals = totals + s[2 * lines :] * factor
    reads = weighted / totals
    diff = reads[:heads] - lambda_ref[...] * reads[heads : 2 * heads]
    mean = jnp.mean(diff * diff, axis=-1, keepdims=True)
    normed = diff * lax.rsqrt(mean + 1e-06) * gain_ref[...]
    headed = jnp.concatenate([normed[h : h + 1] for h in range(heads)], axis=1).astype(BF16)
    width = w_ref.shape[1] // parts
    for b in range(parts):
        board[b] = jnp.dot(
            headed, w_ref[:, pl.ds(b * width, width)], preferred_element_type=F32
        )
    for k in range(parts):
        outs[k][...] = board[lax.rem(me + k, parts)].astype(BF16)


def finish(states, lambdas, gain, out_weight, heads, parts):
    vmem = pl.BlockSpec(memory_space=pltpu.VMEM)
    groups = [s.shape[0] for s in states]
    width = out_weight.shape[1] // parts
    return pl.pallas_call(
        functools.partial(finish_kernel, groups, heads, parts),
        name="finish",
        in_specs=[vmem] * (len(states) + 3),
        out_specs=[vmem] * parts,
        out_shape=[jax.ShapeDtypeStruct((1, width), BF16)] * parts,
        scratch_shapes=[pltpu.VMEM((parts, 1, width), F32)],
        compiler_params=pltpu.CompilerParams(vmem_limit_bytes=16 * 1024 * 1024),
        cost_estimate=pl.CostEstimate(
            flops=2 * out_weight.size, transcendentals=0, bytes_accessed=2 * out_weight.size
        ),
    )(*states, lambdas, gain, out_weight)


def split_rows(rows):
    last = max(16, rows // 4 // 16 * 16)
    if rows % 16 or rows <= 2 * last:
        return [rows]
    return [rows - last, last]


def on_device(axes, layer_input, key_weight, value_weight, new_queries, lambdas, head_gain, out_weight):
    n_sp, n_tp = axes
    heads = lambdas.shape[0]
    columns = key_weight.shape[1]
    head_dim = columns // (2 * heads)
    own = layer_input[0]
    rows = own.shape[0]
    all_rows = rows * n_tp
    first_position = lax.axis_index("sp") * all_rows
    table = rope_table(first_position, all_rows, head_dim)
    paired = n_tp % 2 == 0

    def send(value, move, axis="tp", size=n_tp):
        return lax.ppermute(value, axis, [(i, move(i)) for i in range(size)])

    chunks = split_rows(rows)
    firsts = [sum(chunks[:i]) for i in range(len(chunks))]
    stride = 2 if paired else 1
    hops = range(stride, n_tp, stride)
    crossed = []
    for row, length in zip(firsts, chunks):
        part = own[row : row + length]
        for hop in hops:
            got = send(part, lambda i, hop=hop: (i + hop) % n_tp)
            crossed.append((got, hop, row, length))
    sides = [(own, lambda me: me, 0, rows, rows)]
    if paired:
        sides.append((send(own, lambda i: i ^ 1), lambda me: me ^ 1, 0, rows, rows))
    stages = [sides]
    for row, length in zip(firsts, chunks):
        stage = []
        for got, hop, at, size in crossed:
            if at != row:
                continue
            stage.append((got, lambda me, hop=hop: lax.rem(me + n_tp - hop, n_tp), row, length, rows))
            if paired:
                relayed = send(got, lambda i: i ^ 1)
                stage.append(
                    (relayed, lambda me, hop=hop: lax.rem((me ^ 1) + n_tp - hop, n_tp), row, length, rows)
                )
        if stage:
            stages.append(stage)
    carried = None
    for stage in stages:
        carried = project(
            [piece[0] for piece in stage],
            [piece[1:] for piece in stage],
            key_weight,
            value_weight,
            new_queries,
            table,
            heads,
            head_dim,
            all_rows,
            carried,
        )
    state, keys, values = carried
    state = state[None]
    if n_sp <= 4:
        states = [state] + [
            send(state, lambda i, k=k: (i + k) % n_sp, "sp", n_sp) for k in range(1, n_sp)
        ]
    else:
        states = [lax.all_gather(state, "sp", axis=0, tiled=True)]
    lambda_rows = jnp.broadcast_to(lambdas[:, None], (heads, 2 * head_dim))
    parts = finish(states, lambda_rows, head_gain[None], out_weight, heads, n_tp)
    mixed = parts[0].astype(F32)
    for k in range(1, n_tp):
        mixed = mixed + send(parts[k], lambda i, k=k: (i + k) % n_tp).astype(F32)
    return keys[None], values[None], mixed.astype(BF16)


def solution(mesh):
    in_specs = (
        P("gr", ("sp", "tp"), None),
        P(None, "tp"),
        P(None, "tp"),
        P("gr", "tp"),
        P("tp"),
        P(),
        P("tp", None),
    )
    out_specs = (P("gr", "sp", "tp"), P("gr", "sp", "tp"), P("gr", "tp"))

    def body(*arrays):
        return on_device((mesh.shape["sp"], mesh.shape["tp"]), *arrays)

    return jax.shard_map(
        body, mesh=mesh, in_specs=in_specs, out_specs=out_specs, check_vma=False
    )
```

profile of v0, /device:TPU:0, one launch (start us, length us, event | category | flops | bytes accessed | tf_op | source)
XLA Modules:
  0.0 45.6 jit_solution(6972893059479398184)
XLA Ops:
  0.7 2.1 %slice_bitcast_fusion = bf16[144,2048]{1,0:T(8,128)(2,1)} fusion(bf16[1,192,2048]{2,1,0:T(8,128)(2,1)} %param.7), kind=kLoop, calls=%fused_computation | loop fusion | bytes 1179648 | tf_op jit(solution)/shard_map/slice | solution.py:244
  2.7 3.0 %collective-permute-start.2 = (bf16[144,2048]{1,0:T(8,128)(2,1)}, bf16[144,2048]{1,0:T(8,128)(2,1)S(1)}, u32[]{:S(2)}, u32[]{:S(2)}) collective-permute-start(bf16[144,2048]{1,0:T(8,128)(2,1)} %slice_bitcast_fusion), channel_id=1, source_target_pairs={{0,2},{1,3},{2,0},{3,1},{4,6},{5,7},{6,4},{7,5},{8,10},{9,11},{10,... | collective-permute-start | bytes 1769480 | tf_op jit(solution)/shard_map/ppermute | solution.py:236
  5.7 1.6 %slice_bitcast_fusion.1 = bf16[48,2048]{1,0:T(8,128)(2,1)} fusion(bf16[1,192,2048]{2,1,0:T(8,128)(2,1)} %param.7), kind=kLoop, calls=%fused_computation.4 | loop fusion | bytes 393216 | tf_op jit(solution)/shard_map/slice | solution.py:244
  7.3 12.8 %collective-permute-done.2.refs_0_ = bf16[144,2048]{1,0:T(8,128)(2,1)S(1)} collective-permute-done((bf16[144,2048]{1,0:T(8,128)(2,1)}, bf16[144,2048]{1,0:T(8,128)(2,1)S(1)}, u32[]{:S(2)}, u32[]{:S(2)}) %collective-permute-start.2) | collective-permute-done | bytes 589856 | tf_op jit(solution)/shard_map/ppermute | solution.py:236
  20.1 1.5 %multiply_cosine_fusion = (f32[768,32]{1,0:T(8,128)S(1)}, f32[768,32]{1,0:T(8,128)S(1)}, f32[768,32]{1,0:T(8,128)S(1)}) fusion(f32[768]{0:T(1024)S(1)} %add_convert_fusion, f32[32]{0:T(128)S(1)} %negate_power_fusion), kind=kLoop, calls=%fused_computation.2 | loop fusion | flops 49152 | bytes 298112 | tf_op jit(solution)/shard_map/cos | solution.py:20
  21.6 0.4 pad_maximum_fusion.refs_5_
  21.9 1.6 %collective-permute-done.refs_0_ = bf16[48,2048]{1,0:T(8,128)(2,1)} collective-permute-done((bf16[48,2048]{1,0:T(8,128)(2,1)}, bf16[48,2048]{1,0:T(8,128)(2,1)}, u32[]{:S(2)}, u32[]{:S(2)}) %collective-permute-start) | collective-permute-done | bytes 196640 | tf_op jit(solution)/shard_map/ppermute | solution.py:236
  23.6 1.1 %copy-done.2 = bf16[1,192,2048]{2,1,0:T(8,128)(2,1)S(1)} copy-done((bf16[1,192,2048]{2,1,0:T(8,128)(2,1)S(1)}, bf16[1,192,2048]{2,1,0:T(8,128)(2,1)}, u32[]{:S(2)}) %copy-start.2) | copy-done | bytes 786456
  24.7 2.6 %shard_map.94 = (bf16[768,512]{1,0:T(8,128)(2,1)}, bf16[768,512]{1,0:T(8,128)(2,1)}, f32[24,128]{1,0:T(8,128)S(1)}) custom-call(bf16[192,2048]{1,0:T(8,128)(2,1)S(1)} %bitcast.10, bf16[192,2048]{1,0:T(8,128)(2,1)S(1)} %collective-permute-done.4.refs_1_, bf16[2048,512]{1,0:T(8,128)(2,1)S(1)} %copy-done, bf16[2048,512]{1,0:T(8,128)(2,1)S(1)} %copy-done.1, ...), custom_call_target="tpu_custom_call" | custom-call | flops 1610612736 | bytes 6553600 | tf_op jit(solution)/shard_map/pallas_call | solution.py:148
  27.3 2.1 %shard_map.95 = (bf16[768,512]{1,0:T(8,128)(2,1)}, bf16[768,512]{1,0:T(8,128)(2,1)}, f32[24,128]{1,0:T(8,128)S(1)}) custom-call(bf16[144,2048]{1,0:T(8,128)(2,1)S(1)} %collective-permute-done.2.refs_0_, bf16[144,2048]{1,0:T(8,128)(2,1)S(1)} %collective-permute-done.3.refs_1_, ...), custom_call_target="tpu_custom_call", output_to_operand_aliasing={{0}: (7, {}), {1}: (8, {})} | custom-call | flops 1207959552 | bytes 5963776 | tf_op jit(solution)/shard_map/pallas_call | solution.py:148
  29.5 2.5 %shard_map.96 = (bf16[768,512]{1,0:T(8,128)(2,1)}, bf16[768,512]{1,0:T(8,128)(2,1)}, f32[24,128]{1,0:T(8,128)S(1)}) custom-call(bf16[48,2048]{1,0:T(8,128)(2,1)} %collective-permute-done.refs_0_, bf16[48,2048]{1,0:T(8,128)(2,1)S(1)} %collective-permute-done.1.refs_1_, bf16[2048,512]{1,0:T(8,128)(2,1)S(1)} %copy-done, ...), custom_call_target="tpu_custom_call", output_to_operand_aliasing={{0}: (7, {}), {1}: (8, {})} | custom-call | flops 402653184 | bytes 4784128 | tf_op jit(solution)/shard_map/pallas_call | solution.py:148
  32.1 1.9 %collective-permute-start.5 = (f32[1,24,128]{2,1,0:T(8,128)S(1)}, f32[1,24,128]{2,1,0:T(8,128)S(1)}, u32[]{:S(2)}, u32[]{:S(2)}) collective-permute-start(f32[1,24,128]{2,1,0:T(8,128)S(1)} %bitcast.11), channel_id=1, source_target_pairs={{0,4},{4,8},{8,12},{12,0},{1,5},{5,9},{9,13},{13,1},{2,6},{6,10},{... | collective-permute-start | bytes 36872 | tf_op jit(solution)/shard_map/ppermute | solution.py:236
  34.0 2.6 %collective-permute-start.6 = (f32[1,24,128]{2,1,0:T(8,128)S(1)}, f32[1,24,128]{2,1,0:T(8,128)S(1)}, u32[]{:S(2)}, u32[]{:S(2)}) collective-permute-start(f32[1,24,128]{2,1,0:T(8,128)S(1)} %bitcast.12), channel_id=1, source_target_pairs={{0,8},{4,12},{8,0},{12,4},{1,9},{5,13},{9,1},{13,5},{2,10},{6,14},... | collective-permute-start | bytes 36872 | tf_op jit(solution)/shard_map/ppermute | solution.py:236
  36.6 1.4 %collective-permute-start.7 = (f32[1,24,128]{2,1,0:T(8,128)S(1)}, f32[1,24,128]{2,1,0:T(8,128)S(1)}, u32[]{:S(2)}, u32[]{:S(2)}) collective-permute-start(f32[1,24,128]{2,1,0:T(8,128)S(1)} %bitcast.13), channel_id=1, source_target_pairs={{0,12},{4,0},{8,4},{12,8},{1,13},{5,1},{9,5},{13,9},{2,14},{6,2},{... | collective-permute-start | bytes 36872 | tf_op jit(solution)/shard_map/ppermute | solution.py:236
  37.9 0.7 %collective-permute-done.6.refs_2_ = f32[1,24,128]{2,1,0:T(8,128)S(1)} collective-permute-done((f32[1,24,128]{2,1,0:T(8,128)S(1)}, f32[1,24,128]{2,1,0:T(8,128)S(1)}, u32[]{:S(2)}, u32[]{:S(2)}) %collective-permute-start.6) | collective-permute-done | bytes 12320 | tf_op jit(solution)/shard_map/ppermute | solution.py:236
  38.6 1.7 %collective-permute-done.7.refs_3_ = f32[1,24,128]{2,1,0:T(8,128)S(1)} collective-permute-done((f32[1,24,128]{2,1,0:T(8,128)S(1)}, f32[1,24,128]{2,1,0:T(8,128)S(1)}, u32[]{:S(2)}, u32[]{:S(2)}) %collective-permute-start.7) | collective-permute-done | bytes 12320 | tf_op jit(solution)/shard_map/ppermute | solution.py:236
  40.3 0.1 broadcast_in_dim.23.refs_4_
  40.3 0.5 %finish.1 = (bf16[1,512]{1,0:T(2,128)(2,1)S(1)}, bf16[1,512]{1,0:T(2,128)(2,1)S(1)}, bf16[1,512]{1,0:T(2,128)(2,1)S(1)}, bf16[1,512]{1,0:T(2,128)(2,1)S(1)}) custom-call(f32[1,24,128]{2,1,0:T(8,128)S(1)} %bitcast.14, f32[1,24,128]{2,1,0:T(8,128)S(1)} %collective-permute-done.5.refs_1_, f32[1,24,128]{2,1,0:T(8,128)S(1)} %collective-permute-done.6.refs_2_, ...), custom_call_target="tpu_custom_call" | custom-call | flops 2097152 | bytes 2097152 | tf_op jit(solution)/shard_map/finish/pallas_call | solution.py:202
  40.8 0.1 collective-permute-start.10
  40.9 0.5 %collective-permute-start.8 = (bf16[1,512]{1,0:T(2,128)(2,1)S(1)}, bf16[1,512]{1,0:T(2,128)(2,1)S(1)}, u32[]{:S(2)}, u32[]{:S(2)}) collective-permute-start(bf16[1,512]{1,0:T(2,128)(2,1)S(1)} %get-tuple-element.26), channel_id=1, source_target_pairs={{0,1},{1,2},{2,3},{3,0},{4,5},{5,6},{6,7},{7,4},{8,9},{9,10},{10,1... | collective-permute-start | bytes 3080 | tf_op jit(solution)/shard_map/ppermute | solution.py:236
  41.4 1.5 %collective-permute-start.9 = (bf16[1,512]{1,0:T(2,128)(2,1)S(1)}, bf16[1,512]{1,0:T(2,128)(2,1)S(1)}, u32[]{:S(2)}, u32[]{:S(2)}) collective-permute-start(bf16[1,512]{1,0:T(2,128)(2,1)S(1)} %get-tuple-element.27), channel_id=1, source_target_pairs={{0,2},{1,3},{2,0},{3,1},{4,6},{5,7},{6,4},{7,5},{8,10},{9,11},{10,... | collective-permute-start | bytes 3080 | tf_op jit(solution)/shard_map/ppermute | solution.py:236
  42.9 1.1 %collective-permute-done.8 = bf16[1,512]{1,0:T(2,128)(2,1)S(1)} collective-permute-done((bf16[1,512]{1,0:T(2,128)(2,1)S(1)}, bf16[1,512]{1,0:T(2,128)(2,1)S(1)}, u32[]{:S(2)}, u32[]{:S(2)}) %collective-permute-start.8) | collective-permute-done | bytes 1056 | tf_op jit(solution)/shard_map/ppermute | solution.py:236
  44.0 1.0 %collective-permute-done.9 = bf16[1,512]{1,0:T(2,128)(2,1)S(1)} collective-permute-done((bf16[1,512]{1,0:T(2,128)(2,1)S(1)}, bf16[1,512]{1,0:T(2,128)(2,1)S(1)}, u32[]{:S(2)}, u32[]{:S(2)}) %collective-permute-start.9) | collective-permute-done | bytes 1056 | tf_op jit(solution)/shard_map/ppermute | solution.py:236
  45.0 0.6 %add_convert_fusion.1 = bf16[1,512]{1,0:T(2,128)(2,1)} fusion(bf16[1,512]{1,0:T(2,128)(2,1)S(1)} %collective-permute-done.10, bf16[1,512]{1,0:T(2,128)(2,1)S(1)} %collective-permute-done.9, bf16[1,512]{1,0:T(2,128)(2,1)S(1)} %collective-permute-done.8, bf16[1,512]{1,0:T(2,128)(2,1)S(1)} %get-tuple-element.25), kind=kLoop, calls=%fused_computation.7 | loop fusion | flops 4096 | bytes 5120 | tf_op jit(solution)/shard_map/convert_element_type | solution.py:292
  (24 shorter events, 0.1 us)
Async XLA Ops:
  0.6 22.9 %copy-start.4 = (bf16[1,512]{1,0:T(2,128)(2,1)S(1)}, bf16[1,512]{1,0:T(2,128)(2,1)}, u32[]{:S(2)}) copy-start(bf16[1,512]{1,0:T(2,128)(2,1)} %refs_4_.5) | copy-start | bytes 3076
  0.6 22.9 %copy-start = (bf16[2048,512]{1,0:T(8,128)(2,1)S(1)}, bf16[2048,512]{1,0:T(8,128)(2,1)}, u32[]{:S(2)}) copy-start(bf16[2048,512]{1,0:T(8,128)(2,1)} %refs_2_.5) | copy-start | bytes 6291460
  2.7 17.4 %collective-permute-start.2 = (bf16[144,2048]{1,0:T(8,128)(2,1)}, bf16[144,2048]{1,0:T(8,128)(2,1)S(1)}, u32[]{:S(2)}, u32[]{:S(2)}) collective-permute-start(bf16[144,2048]{1,0:T(8,128)(2,1)} %slice_bitcast_fusion), channel_id=1, source_target_pairs={{0,2},{1,3},{2,0},{3,1},{4,6},{5,7},{6,4},{7,5},{8,10},{9,11},{10,... | collective-permute-start | bytes 1769480 | tf_op jit(solution)/shard_map/ppermute | solution.py:236
  5.7 17.9 %collective-permute-start.4 = (bf16[192,2048]{1,0:T(8,128)(2,1)}, bf16[192,2048]{1,0:T(8,128)(2,1)S(1)}, u32[]{:S(2)}, u32[]{:S(2)}) collective-permute-start(bf16[192,2048]{1,0:T(8,128)(2,1)} %bitcast.9), channel_id=1, source_target_pairs={{0,1},{1,0},{2,3},{3,2},{4,5},{5,4},{6,7},{7,6},{8,9},{9,8},{10,11... | collective-permute-start | bytes 2359304 | tf_op jit(solution)/shard_map/ppermute | solution.py:236
  7.3 16.2 %collective-permute-start = (bf16[48,2048]{1,0:T(8,128)(2,1)}, bf16[48,2048]{1,0:T(8,128)(2,1)}, u32[]{:S(2)}, u32[]{:S(2)}) collective-permute-start(bf16[48,2048]{1,0:T(8,128)(2,1)} %slice_bitcast_fusion.1), channel_id=1, source_target_pairs={{0,2},{1,3},{2,0},{3,1},{4,6},{5,7},{6,4},{7,5},{8,10},{9,11},{10,... | collective-permute-start | bytes 589832 | tf_op jit(solution)/shard_map/ppermute | solution.py:236
  7.3 16.3 %copy-start.1 = (bf16[2048,512]{1,0:T(8,128)(2,1)S(1)}, bf16[2048,512]{1,0:T(8,128)(2,1)}, u32[]{:S(2)}) copy-start(bf16[2048,512]{1,0:T(8,128)(2,1)} %refs_3_.5) | copy-start | bytes 6291460
  20.1 7.2 %collective-permute-start.3 = (bf16[144,2048]{1,0:T(8,128)(2,1)S(1)}, bf16[144,2048]{1,0:T(8,128)(2,1)S(1)}, u32[]{:S(2)}, u32[]{:S(2)}) collective-permute-start(bf16[144,2048]{1,0:T(8,128)(2,1)S(1)} %collective-permute-done.2.refs_0_), channel_id=1, source_target_pairs={{0,1},{1,0},{2,3},{3,2},{4,5},{5,4},{6,7},{7,6},{8,9},{9,8},{10,11... | collective-permute-start | bytes 1769480 | tf_op jit(solution)/shard_map/ppermute | solution.py:236
  23.6 5.9 %collective-permute-start.1 = (bf16[48,2048]{1,0:T(8,128)(2,1)}, bf16[48,2048]{1,0:T(8,128)(2,1)S(1)}, u32[]{:S(2)}, u32[]{:S(2)}) collective-permute-start(bf16[48,2048]{1,0:T(8,128)(2,1)} %collective-permute-done.refs_0_), channel_id=1, source_target_pairs={{0,1},{1,0},{2,3},{3,2},{4,5},{5,4},{6,7},{7,6},{8,9},{9,8},{10,11... | collective-permute-start | bytes 589832 | tf_op jit(solution)/shard_map/ppermute | solution.py:236
  23.6 1.1 %copy-start.2 = (bf16[1,192,2048]{2,1,0:T(8,128)(2,1)S(1)}, bf16[1,192,2048]{2,1,0:T(8,128)(2,1)}, u32[]{:S(2)}) copy-start(bf16[1,192,2048]{2,1,0:T(8,128)(2,1)} %param.7) | copy-start | bytes 2359300
  29.5 10.8 %copy-start.6 = (f32[4]{0:T(128)S(1)}, f32[4]{0:T(128)}, u32[]{:S(2)}) copy-start(f32[4]{0:T(128)} %param.11) | copy-start | bytes 52
  29.5 10.8 %copy-start.3 = (bf16[512,2048]{1,0:T(8,128)(2,1)S(1)}, bf16[512,2048]{1,0:T(8,128)(2,1)}, u32[]{:S(2)}) copy-start(bf16[512,2048]{1,0:T(8,128)(2,1)} %refs_6_.1) | copy-start | bytes 6291460
  29.5 10.8 %copy-start.5 = (f32[128]{0:T(128)S(1)}, f32[128]{0:T(128)}, u32[]{:S(2)}) copy-start(f32[128]{0:T(128)} %param.12) | copy-start | bytes 1540
  32.1 5.8 %collective-permute-start.5 = (f32[1,24,128]{2,1,0:T(8,128)S(1)}, f32[1,24,128]{2,1,0:T(8,128)S(1)}, u32[]{:S(2)}, u32[]{:S(2)}) collective-permute-start(f32[1,24,128]{2,1,0:T(8,128)S(1)} %bitcast.11), channel_id=1, source_target_pairs={{0,4},{4,8},{8,12},{12,0},{1,5},{5,9},{9,13},{13,1},{2,6},{6,10},{... | collective-permute-start | bytes 36872 | tf_op jit(solution)/shard_map/ppermute | solution.py:236
  34.0 4.6 %collective-permute-start.6 = (f32[1,24,128]{2,1,0:T(8,128)S(1)}, f32[1,24,128]{2,1,0:T(8,128)S(1)}, u32[]{:S(2)}, u32[]{:S(2)}) collective-permute-start(f32[1,24,128]{2,1,0:T(8,128)S(1)} %bitcast.12), channel_id=1, source_target_pairs={{0,8},{4,12},{8,0},{12,4},{1,9},{5,13},{9,1},{13,5},{2,10},{6,14},... | collective-permute-start | bytes 36872 | tf_op jit(solution)/shard_map/ppermute | solution.py:236
  36.6 3.7 %collective-permute-start.7 = (f32[1,24,128]{2,1,0:T(8,128)S(1)}, f32[1,24,128]{2,1,0:T(8,128)S(1)}, u32[]{:S(2)}, u32[]{:S(2)}) collective-permute-start(f32[1,24,128]{2,1,0:T(8,128)S(1)} %bitcast.13), channel_id=1, source_target_pairs={{0,12},{4,0},{8,4},{12,8},{1,13},{5,1},{9,5},{13,9},{2,14},{6,2},{... | collective-permute-start | bytes 36872 | tf_op jit(solution)/shard_map/ppermute | solution.py:236
  40.8 2.1 %collective-permute-start.10 = (bf16[1,512]{1,0:T(2,128)(2,1)S(1)}, bf16[1,512]{1,0:T(2,128)(2,1)S(1)}, u32[]{:S(2)}, u32[]{:S(2)}) collective-permute-start(bf16[1,512]{1,0:T(2,128)(2,1)S(1)} %get-tuple-element.28), channel_id=1, source_target_pairs={{0,3},{1,0},{2,1},{3,2},{4,7},{5,4},{6,5},{7,6},{8,11},{9,8},{10,9... | collective-permute-start | bytes 3080 | tf_op jit(solution)/shard_map/ppermute | solution.py:236
  40.9 3.1 %collective-permute-start.8 = (bf16[1,512]{1,0:T(2,128)(2,1)S(1)}, bf16[1,512]{1,0:T(2,128)(2,1)S(1)}, u32[]{:S(2)}, u32[]{:S(2)}) collective-permute-start(bf16[1,512]{1,0:T(2,128)(2,1)S(1)} %get-tuple-element.26), channel_id=1, source_target_pairs={{0,1},{1,2},{2,3},{3,0},{4,5},{5,6},{6,7},{7,4},{8,9},{9,10},{10,1... | collective-permute-start | bytes 3080 | tf_op jit(solution)/shard_map/ppermute | solution.py:236
  41.4 3.6 %collective-permute-start.9 = (bf16[1,512]{1,0:T(2,128)(2,1)S(1)}, bf16[1,512]{1,0:T(2,128)(2,1)S(1)}, u32[]{:S(2)}, u32[]{:S(2)}) collective-permute-start(bf16[1,512]{1,0:T(2,128)(2,1)S(1)} %get-tuple-element.27), channel_id=1, source_target_pairs={{0,2},{1,3},{2,0},{3,1},{4,6},{5,7},{6,4},{7,5},{8,10},{9,11},{10,... | collective-permute-start | bytes 3080 | tf_op jit(solution)/shard_map/ppermute | solution.py:236
where the time goes:
time: 45.8 us; the launch traced here: 45.6 us
  waiting for transfers between devices  18.8 us (41%)
  starting transfers between devices  10.9 us (24%)
  Pallas kernels  7.76 us (17%)
  local copies, waits for them, and re-layouts  4.92 us (11%)
  other arithmetic  2.43 us (5%)
  between operations  0.78 us (2%)
    ppermute x11, waiting for transfers between devices, send(): return lax.ppermute(value, axis, [(i, move(i)) for i in range(size)])  18.8 us
    ppermute x11, starting transfers between devices, send(): return lax.ppermute(value, axis, [(i, move(i)) for i in range(size)])  10.9 us
    pallas_call x3, Pallas kernels, project(): pl.pallas_call(functools.partial(project_kernel, pieces, heads, head_dim,...  7.28 us
    slice x2, local copies, waits for them, and re-layouts, on_device(): part = own[row:row + length]  3.7 us
    cos x1, other arithmetic, rope_table(): cosine, sine = (jnp.cos(angles), jnp.sin(angles))  1.45 us
    unnamed x14, local copies, waits for them, and re-layouts  1.16 us
  transfers between devices with their start and end apart: 11, of which 6 were waited for; matrix products, arithmetic and copies ran while one was open for 8% of the time, Pallas kernels for 10%

commit v1 on v0

--- a/solution.py
+++ b/solution.py
@@ -9,6 +9,8 @@
 
 
 LANES = 128
+TILE = 512
+MIB = 1024 * 1024
 F32 = jnp.float32
 BF16 = jnp.bfloat16
 
@@ -34,22 +36,70 @@
     return rows * cosine + turned * sine
 
 
-def project_kernel(pieces, heads, head_dim, tile, first, *refs):
+def in_vmem(array):
+    return pltpu.with_memory_space_constraint(array, pltpu.VMEM)
+
+
+def cut_kernel(firsts, lengths, x_ref, *refs):
+    outs, sem = refs[:-1], refs[-1]
+    copies = [
+        pltpu.make_async_copy(x_ref.at[pl.ds(row, length)], out, sem.at[i])
+        for i, (row, length, out) in enumerate(zip(firsts, lengths, outs))
+    ]
+    for copy in copies:
+        copy.start()
+    for copy in copies:
+        copy.wait()
+
+
+def cut(array, firsts, lengths):
+    return pl.pallas_call(
+        functools.partial(cut_kernel, firsts, lengths),
+        in_specs=[pl.BlockSpec(memory_space=pltpu.HBM)],
+        out_specs=[pl.BlockSpec(memory_space=pltpu.VMEM)] * len(firsts),
+        out_shape=[pltpu.VMEM((n, array.shape[1]), array.dtype) for n in lengths],
+        scratch_shapes=[pltpu.SemaphoreType.DMA((len(firsts),))],
+        compiler_params=pltpu.CompilerParams(vmem_limit_bytes=MIB),
+    )(pltpu.with_memory_space_constraint(array, pltpu.HBM))
+
+
+def row_offsets(pieces):
+    me = lax.axis_index("tp")
+    return [pl.multiple_of(source(me) * block + row, 16) for source, row, _, block in pieces]
+
+
+def write_out(pieces, offsets, buffers, outs, sem):
+    copies, at = [], 0
+    for offset, (_, _, length, _) in zip(offsets, pieces):
+        for buffer, out in zip(buffers, outs):
+            copies.append(
+                pltpu.make_async_copy(
+                    buffer.at[pl.ds(at, length)], out.at[pl.ds(offset, length)], sem.at[len(copies)]
+                )
+            )
+        at += length
+    for copy in copies:
+        copy.start()
+    return copies
+
+
+def project_kernel(pieces, heads, head_dim, tile, first, last, *refs):
     count = len(pieces)
     x_refs, refs = refs[:count], refs[count:]
     wk_ref, wv_ref, q_ref, table_ref, refs = refs[0], refs[1], refs[2], refs[3], refs[4:]
     if not first:
-        before_ref, refs = refs[0], refs[3:]
-    k_out, v_out, state_ref, xs, kbuf, vbuf, o_sem = refs
-    me = lax.axis_index("tp")
-    block_rows = pieces[0][3]
+        before_ref, refs = refs[0], refs[1:]
+    if not last:
+        if not first:
+            refs = refs[2:]
+        k_out, v_out, state_ref, xs, kbuf, vbuf, k_sem, v_sem = refs
+    else:
+        kbuf, vbuf, state_ref, xs = refs
     columns = wk_ref.shape[1]
     lengths = [piece[2] for piece in pieces]
     starts = [sum(lengths[:i]) for i in range(count)]
     total = sum(lengths)
-    offsets = [
-        pl.multiple_of(source(me) * block_rows + row, 16) for source, row, _, _ in pieces
-    ]
+    offsets = row_offsets(pieces)
     if count > 1 and total <= xs.shape[0]:
         for i in range(count):
             xs[pl.ds(starts[i], lengths[i]), :] = x_refs[i][...]
@@ -58,17 +108,7 @@
         spans = [(x_refs[i], starts[i], lengths[i]) for i in range(count)]
     tables = [table_ref[pl.ds(offsets[i], lengths[i]), :] for i in range(count)]
     table = tables[0] if count == 1 else jnp.concatenate(tables, axis=0)
-
-    def writes(buffer, out, base):
-        return [
-            pltpu.make_async_copy(
-                buffer.at[pl.ds(starts[i], lengths[i])],
-                out.at[pl.ds(offsets[i], lengths[i])],
-                o_sem.at[base + i],
-            )
-            for i in range(count)
-        ]
-
+    copies = []
     for c in range(0, columns, tile):
         for x_ref, row, length in spans:
             raw = jnp.dot(
@@ -77,18 +117,16 @@
             for d in range(0, tile, LANES):
                 turned = turn(raw[:, d : d + LANES], table[row : row + length], head_dim)
                 kbuf[pl.ds(row, length), pl.ds(c + d, LANES)] = turned.astype(BF16)
-    k_writes = writes(kbuf, k_out, 0)
-    for copy in k_writes:
-        copy.start()
+    if not last:
+        copies += write_out(pieces, offsets, [kbuf], [k_out], k_sem)
     for c in range(0, columns, tile):
         for x_ref, row, length in spans:
             raw = jnp.dot(
                 x_ref[...], wv_ref[:, pl.ds(c, tile)], preferred_element_type=F32
             )
             vbuf[pl.ds(row, length), pl.ds(c, tile)] = raw.astype(BF16)
-    v_writes = writes(vbuf, v_out, count)
-    for copy in v_writes:
-        copy.start()
+    if not last:
+        copies += write_out(pieces, offsets, [vbuf], [v_out], v_sem)
 
     lines = state_ref.shape[0] // 3
     line = lax.broadcasted_iota(jnp.int32, (lines, columns), 0)
@@ -123,51 +161,74 @@
     state_ref[pl.ds(0, lines), :] = weighted
     state_ref[pl.ds(lines, lines), :] = jnp.broadcast_to(highest, (lines, 2 * head_dim))
     state_ref[pl.ds(2 * lines, lines), :] = jnp.broadcast_to(totals, (lines, 2 * head_dim))
-    for copy in k_writes + v_writes:
+    for copy in copies:
         copy.wait()
 
 
-def project(arrays, pieces, wk, wv, queries, table, heads, head_dim, all_rows, carried):
+def project(arrays, pieces, wk, wv, queries, table, heads, head_dim, all_rows, carried, last):
     depth, columns = wk.shape
-    tile = min(256, columns)
     total = sum(piece[2] for piece in pieces)
     lines = max(8, 2 * heads)
     count = len(pieces)
     anywhere = pl.BlockSpec(memory_space=pltpu.HBM)
     vmem = pl.BlockSpec(memory_space=pltpu.VMEM)
     first = carried is None
-    operands = [*arrays, wk, wv, queries, table]
-    in_specs = [vmem] * (count + 4)
+    operands = [in_vmem(a) for a in (*arrays, wk, wv, queries, table)]
     aliases = {}
     if not first:
-        state, keys, values = carried
-        operands += [state, keys, values]
-        in_specs += [vmem, anywhere, anywhere]
-        aliases = {count + 5: 0, count + 6: 1}
-    cache = jax.ShapeDtypeStruct((all_rows, columns), BF16)
-    keys, values, state = pl.pallas_call(
-        functools.partial(project_kernel, pieces, heads, head_dim, tile, first),
+        operands.append(in_vmem(carried[0]))
+    in_specs = [vmem] * len(operands)
+    own = [pltpu.VMEM((total, columns), BF16)] * 2
+    sems = [pltpu.SemaphoreType.DMA((count,))] * 2
+    state_shape = jax.ShapeDtypeStruct((3 * lines, 2 * head_dim), F32)
+    if last:
+        rows_shape = jax.ShapeDtypeStruct((total, columns), BF16)
+        own, sems = [], []
+    else:
+        rows_shape = jax.ShapeDtypeStruct((all_rows, columns), BF16)
+        if not first:
+            aliases = {len(operands): 0, len(operands) + 1: 1}
+            operands += carried[1:]
+            in_specs += [anywhere] * 2
+    return pl.pallas_call(
+        functools.partial(project_kernel, pieces, heads, head_dim, min(TILE, columns), first, last),
         in_specs=in_specs,
-        out_specs=[anywhere, anywhere, vmem],
-        out_shape=[cache, cache, jax.ShapeDtypeStruct((3 * lines, 2 * head_dim), F32)],
+        out_specs=[vmem if last else anywhere] * 2 + [vmem],
+        out_shape=[rows_shape, rows_shape, state_shape],
         input_output_aliases=aliases,
-        scratch_shapes=[
-            pltpu.VMEM((min(total, 256) if count > 1 else 16, depth), BF16),
-            pltpu.VMEM((total, columns), BF16),
-            pltpu.VMEM((total, columns), BF16),
-            pltpu.SemaphoreType.DMA((2 * count,)),
-        ],
-        compiler_params=pltpu.CompilerParams(vmem_limit_bytes=32 * 1024 * 1024),
+        scratch_shapes=[pltpu.VMEM((min(total, 256) if count > 1 else 16, depth), BF16), *own, *sems],
+        compiler_params=pltpu.CompilerParams(vmem_limit_bytes=12 * MIB),
         cost_estimate=pl.CostEstimate(
             flops=4 * total * depth * columns,
             transcendentals=0,
             bytes_accessed=4 * depth * columns + 2 * total * (depth + 2 * columns),
         ),
     )(*operands)
-    return state, keys, values
-
-
-def finish_kernel(groups, heads, parts, *refs):
+
+
+def store_kernel(pieces, k_rows, v_rows, k_in, v_in, k_out, v_out, sem):
+    copies = write_out(pieces, row_offsets(pieces), [k_rows, v_rows], [k_out, v_out], sem)
+    for copy in copies:
+        copy.wait()
+
+
+def store(pieces, k_rows, v_rows, keys, values):
+    anywhere = pl.BlockSpec(memory_space=pltpu.HBM)
+    vmem = pl.BlockSpec(memory_space=pltpu.VMEM)
+    cache = jax.ShapeDtypeStruct(keys.shape, keys.dtype)
+    return pl.pallas_call(
+        functools.partial(store_kernel, pieces),
+        name="store",
+        in_specs=[vmem, vmem, anywhere, anywhere],
+        out_specs=[anywhere, anywhere],
+        out_shape=[cache, cache],
+        input_output_aliases={2: 0, 3: 1},
+        scratch_shapes=[pltpu.SemaphoreType.DMA((2 * len(pieces),))],
+        compiler_params=pltpu.CompilerParams(vmem_limit_bytes=MIB),
+    )(k_rows, v_rows, keys, values)
+
+
+def finish_kernel(groups, heads, parts, moves, *refs):
     state_refs = refs[: len(groups)]
     lambda_ref, gain_ref, w_ref = refs[len(groups) : len(groups) + 3]
     outs = refs[len(groups) + 3 : len(groups) + 3 + parts]
@@ -191,16 +252,17 @@
         board[b] = jnp.dot(
             headed, w_ref[:, pl.ds(b * width, width)], preferred_element_type=F32
         )
-    for k in range(parts):
-        outs[k][...] = board[lax.rem(me + k, parts)].astype(BF16)
-
-
-def finish(states, lambdas, gain, out_weight, heads, parts):
+    outs[0][...] = board[me].astype(BF16)
+    for out, move in zip(outs[1:], moves):
+        out[...] = board[move(me)].astype(BF16)
+
+
+def finish(states, lambdas, gain, out_weight, heads, parts, moves):
     vmem = pl.BlockSpec(memory_space=pltpu.VMEM)
     groups = [s.shape[0] for s in states]
     width = out_weight.shape[1] // parts
     return pl.pallas_call(
-        functools.partial(finish_kernel, groups, heads, parts),
+        functools.partial(finish_kernel, groups, heads, parts, moves),
         name="finish",
         in_specs=[vmem] * (len(states) + 3),
         out_specs=[vmem] * parts,
@@ -210,14 +272,20 @@
         cost_estimate=pl.CostEstimate(
             flops=2 * out_weight.size, transcendentals=0, bytes_accessed=2 * out_weight.size
         ),
-    )(*states, lambdas, gain, out_weight)
+    )(*[in_vmem(a) for a in (*states, lambdas, gain, out_weight)])
 
 
 def split_rows(rows):
-    last = max(16, rows // 4 // 16 * 16)
-    if rows % 16 or rows <= 2 * last:
+    first, last = rows // 6 // 16 * 16, rows // 4 // 16 * 16
+    if rows % 16 or not first:
         return [rows]
-    return [rows - last, last]
+    return [first, rows - first - last, last]
+
+
+def exchange(count):
+    if count & (count - 1) == 0:
+        return [lambda i, k=k: i ^ k for k in range(1, count)]
+    return [lambda i, k=k: (i + k) % count for k in range(1, count)]
 
 
 def on_device(axes, layer_input, key_weight, value_weight, new_queries, lambdas, head_gain, out_weight):
@@ -239,15 +307,18 @@
     firsts = [sum(chunks[:i]) for i in range(len(chunks))]
     stride = 2 if paired else 1
     hops = range(stride, n_tp, stride)
+    cuts = cut(own, firsts[:1], chunks[:1])
+    if len(chunks) > 1:
+        cuts += cut(own, firsts[1:], chunks[1:])
     crossed = []
-    for row, length in zip(firsts, chunks):
-        part = own[row : row + length]
+    for row, length, part in zip(firsts, chunks, cuts):
         for hop in hops:
             got = send(part, lambda i, hop=hop: (i + hop) % n_tp)
             crossed.append((got, hop, row, length))
     sides = [(own, lambda me: me, 0, rows, rows)]
     if paired:
-        sides.append((send(own, lambda i: i ^ 1), lambda me: me ^ 1, 0, rows, rows))
+        sibling = send(own, lambda i: i ^ 1)
+        sides.append((sibling, lambda me: me ^ 1, 0, rows, rows))
     stages = [sides]
     for row, length in zip(firsts, chunks):
         stage = []
@@ -263,8 +334,9 @@
         if stage:
             stages.append(stage)
     carried = None
-    for stage in stages:
-        carried = project(
+    for index, stage in enumerate(stages):
+        last = index > 0 and index == len(stages) - 1
+        got = project(
             [piece[0] for piece in stage],
             [piece[1:] for piece in stage],
             key_weight,
@@ -275,20 +347,30 @@
             head_dim,
             all_rows,
             carried,
+            last,
         )
-    state, keys, values = carried
+        if last:
+            keys, values = carried[1:]
+            state = got[2]
+        else:
+            keys, values, state = got
+            carried = (state, keys, values)
     state = state[None]
     if n_sp <= 4:
-        states = [state] + [
-            send(state, lambda i, k=k: (i + k) % n_sp, "sp", n_sp) for k in range(1, n_sp)
-        ]
+        states = [state]
+        for move in exchange(n_sp):
+            states.append(send(state, move, "sp", n_sp))
     else:
         states = [lax.all_gather(state, "sp", axis=0, tiled=True)]
+    if len(stages) > 1:
+        keys, values = store([piece[1:] for piece in stages[-1]], got[0], got[1], keys, values)
     lambda_rows = jnp.broadcast_to(lambdas[:, None], (heads, 2 * head_dim))
-    parts = finish(states, lambda_rows, head_gain[None], out_weight, heads, n_tp)
-    mixed = parts[0].astype(F32)
-    for k in range(1, n_tp):
-        mixed = mixed + send(parts[k], lambda i, k=k: (i + k) % n_tp).astype(F32)
+    moves = exchange(n_tp)
+    shares = finish(states, lambda_rows, head_gain[None], out_weight, heads, n_tp, moves)
+    mixed = shares[0].astype(F32)
+    for k, move in enumerate(moves):
+        got = send(shares[k + 1], move)
+        mixed = mixed + got.astype(F32)
     return keys[None], values[None], mixed.astype(BF16)
 
 

time: 45.8 us -> 48.7 us (1.063)
  Pallas kernels: 7.76 us -> 12.8 us
  local copies, waits for them, and re-layouts: 4.92 us -> 1.23 us
  waiting for transfers between devices: 18.8 us -> 19.7 us
  starting transfers between devices: 10.9 us -> 11.5 us
    pallas_call x1 -> x4, Pallas kernels: 0.48 us -> 4.8 us  [the longest x2 3.62 us: cut(): pl.pallas_call(functools.partial(cut_kernel, firsts, lengths), in_specs=[...]
    slice x2 -> x0, local copies, waits for them, and re-layouts: 3.7 us -> none  [on_device(): part = own[row:row + length]]
    ppermute x11 -> x13, waiting for transfers between devices: 18.8 us -> 19.7 us  [send(): return lax.ppermute(value, axis, [(i, move(i)) for i in range(size)])]
    pallas_call x3 -> x4, Pallas kernels: 7.28 us -> 8.02 us  [project(): pl.pallas_call(functools.partial(project_kernel, pieces, heads, head_dim,...]
    ppermute x11 -> x13, starting transfers between devices: 10.9 us -> 11.5 us  [send(): return lax.ppermute(value, axis, [(i, move(i)) for i in range(size)])]
  transfers between devices with their start and end apart: 11 -> 13, of which waited for: 6 -> 7; matrix products, arithmetic and copies ran while one was open for 8% -> 4% of each run, Pallas kernels for 10% -> 19%
where the time goes in v1:
time: 48.7 us; the launch traced here: 48.5 us
  waiting for transfers between devices  19.7 us (40%)
  Pallas kernels  12.8 us (26%)
  starting transfers between devices  11.5 us (24%)
  other arithmetic  2.42 us (5%)
  local copies, waits for them, and re-layouts  1.23 us (3%)
  between operations  0.82 us (2%)
    ppermute x13, waiting for transfers between devices, send(): return lax.ppermute(value, axis, [(i, move(i)) for i in range(size)])  19.7 us
    ppermute x13, starting transfers between devices, send(): return lax.ppermute(value, axis, [(i, move(i)) for i in range(size)])  11.5 us
    pallas_call x4, Pallas kernels, project(): pl.pallas_call(functools.partial(project_kernel, pieces, heads, head_dim,...  8.02 us
    pallas_call x2, Pallas kernels, cut(): pl.pallas_call(functools.partial(cut_kernel, firsts, lengths), in_specs=[...  3.62 us
    cos x1, other arithmetic, rope_table(): cosine, sine = (jnp.cos(angles), jnp.sin(angles))  1.44 us
    unnamed x14, local copies, waits for them, and re-layouts  1.16 us
  transfers between devices with their start and end apart: 13, of which 7 were waited for; matrix products, arithmetic and copies ran while one was open for 4% of the time, Pallas kernels for 19%

profile of v1, /device:TPU:0, one launch (start us, length us, event | category | flops | bytes accessed | tf_op | source)
XLA Modules:
  0.0 48.5 jit_solution(8049388312948886348)
XLA Ops:
  0.7 2.1 %shard_map.94 = (bf16[112,2048]{1,0:T(8,128)(2,1)}, bf16[48,2048]{1,0:T(8,128)(2,1)}) custom-call(bf16[192,2048]{1,0:T(8,128)(2,1)} %bitcast.5), custom_call_target="tpu_custom_call" | custom-call | tf_op jit(solution)/shard_map/pallas_call | solution.py:56
  2.7 3.0 %collective-permute-start.2 = (bf16[112,2048]{1,0:T(8,128)(2,1)}, bf16[112,2048]{1,0:T(8,128)(2,1)S(1)}, u32[]{:S(2)}, u32[]{:S(2)}) collective-permute-start(bf16[112,2048]{1,0:T(8,128)(2,1)} %get-tuple-element.24), channel_id=1, source_target_pairs={{0,2},{1,3},{2,0},{3,1},{4,6},{5,7},{6,4},{7,5},{8,10},{9,11},{10,... | collective-permute-start | bytes 1376264 | tf_op jit(solution)/shard_map/ppermute | solution.py:304
  5.8 1.6 %shard_map.95 = bf16[32,2048]{1,0:T(8,128)(2,1)} custom-call(bf16[192,2048]{1,0:T(8,128)(2,1)} %bitcast.7), custom_call_target="tpu_custom_call" | custom-call | tf_op jit(solution)/shard_map/pallas_call | solution.py:56
  7.5 1.9 %collective-permute-start = (bf16[48,2048]{1,0:T(8,128)(2,1)}, bf16[48,2048]{1,0:T(8,128)(2,1)S(1)}, u32[]{:S(2)}, u32[]{:S(2)}) collective-permute-start(bf16[48,2048]{1,0:T(8,128)(2,1)} %get-tuple-element.23), channel_id=1, source_target_pairs={{0,2},{1,3},{2,0},{3,1},{4,6},{5,7},{6,4},{7,5},{8,10},{9,11},{10,... | collective-permute-start | bytes 589832 | tf_op jit(solution)/shard_map/ppermute | solution.py:304
  9.4 7.9 %collective-permute-done.2.refs_0_ = bf16[112,2048]{1,0:T(8,128)(2,1)S(1)} collective-permute-done((bf16[112,2048]{1,0:T(8,128)(2,1)}, bf16[112,2048]{1,0:T(8,128)(2,1)S(1)}, u32[]{:S(2)}, u32[]{:S(2)}) %collective-permute-start.2) | collective-permute-done | bytes 458784 | tf_op jit(solution)/shard_map/ppermute | solution.py:304
  17.3 1.4 %multiply_cosine_fusion = (f32[768,32]{1,0:T(8,128)S(1)}, f32[768,32]{1,0:T(8,128)S(1)}, f32[768,32]{1,0:T(8,128)S(1)}) fusion(f32[768]{0:T(1024)S(1)} %add_convert_fusion, f32[32]{0:T(128)S(1)} %negate_power_fusion), kind=kLoop, calls=%fused_computation.1 | loop fusion | flops 49152 | bytes 298112 | tf_op jit(solution)/shard_map/cos | solution.py:22
  18.8 0.4 pad_maximum_fusion.refs_5_
  19.2 1.1 %collective-permute-done.4.refs_0_ = bf16[32,2048]{1,0:T(8,128)(2,1)} collective-permute-done((bf16[32,2048]{1,0:T(8,128)(2,1)}, bf16[32,2048]{1,0:T(8,128)(2,1)}, u32[]{:S(2)}, u32[]{:S(2)}) %collective-permute-start.4) | collective-permute-done | bytes 131104 | tf_op jit(solution)/shard_map/ppermute | solution.py:304
  20.2 3.3 %collective-permute-done.refs_0_ = bf16[48,2048]{1,0:T(8,128)(2,1)S(1)} collective-permute-done((bf16[48,2048]{1,0:T(8,128)(2,1)}, bf16[48,2048]{1,0:T(8,128)(2,1)S(1)}, u32[]{:S(2)}, u32[]{:S(2)}) %collective-permute-start) | collective-permute-done | bytes 196640 | tf_op jit(solution)/shard_map/ppermute | solution.py:304
  23.5 1.1 %copy-done.2 = bf16[1,192,2048]{2,1,0:T(8,128)(2,1)S(1)} copy-done((bf16[1,192,2048]{2,1,0:T(8,128)(2,1)S(1)}, bf16[1,192,2048]{2,1,0:T(8,128)(2,1)}, u32[]{:S(2)}) %copy-start.2) | copy-done | bytes 786456
  24.7 2.6 %shard_map.96 = (bf16[768,512]{1,0:T(8,128)(2,1)}, bf16[768,512]{1,0:T(8,128)(2,1)}, f32[24,128]{1,0:T(8,128)S(1)}) custom-call(bf16[192,2048]{1,0:T(8,128)(2,1)S(1)} %bitcast.8, bf16[192,2048]{1,0:T(8,128)(2,1)S(1)} %collective-permute-done.6.refs_1_, bf16[2048,512]{1,0:T(8,128)(2,1)S(1)} %copy-done, bf16[2048,512]{1,0:T(8,128)(2,1)S(1)} %copy-done.1, ...), custom_call_target="tpu_custom_call" | custom-call | flops 1610612736 | bytes 6553600 | tf_op jit(solution)/shard_map/pallas_call | solution.py:193
  27.3 2.4 %shard_map.97 = (bf16[768,512]{1,0:T(8,128)(2,1)}, bf16[768,512]{1,0:T(8,128)(2,1)}, f32[24,128]{1,0:T(8,128)S(1)}) custom-call(bf16[32,2048]{1,0:T(8,128)(2,1)} %collective-permute-done.4.refs_0_, bf16[32,2048]{1,0:T(8,128)(2,1)S(1)} %collective-permute-done.5.refs_1_, bf16[2048,512]{1,0:T(8,128)(2,1)S(1)} %copy-done, ...), custom_call_target="tpu_custom_call", output_to_operand_aliasing={{0}: (7, {}), {1}: (8, {})} | custom-call | flops 268435456 | bytes 4587520 | tf_op jit(solution)/shard_map/pallas_call | solution.py:193
  29.7 1.9 %shard_map.98 = (bf16[768,512]{1,0:T(8,128)(2,1)}, bf16[768,512]{1,0:T(8,128)(2,1)}, f32[24,128]{1,0:T(8,128)S(1)}) custom-call(bf16[112,2048]{1,0:T(8,128)(2,1)S(1)} %collective-permute-done.2.refs_0_, bf16[112,2048]{1,0:T(8,128)(2,1)S(1)} %collective-permute-done.3.refs_1_, ...), custom_call_target="tpu_custom_call", output_to_operand_aliasing={{0}: (7, {}), {1}: (8, {})} | custom-call | flops 939524096 | bytes 5570560 | tf_op jit(solution)/shard_map/pallas_call | solution.py:193
  31.6 1.1 %shard_map.99 = (bf16[96,512]{1,0:T(8,128)(2,1)S(1)}, bf16[96,512]{1,0:T(8,128)(2,1)S(1)}, f32[24,128]{1,0:T(8,128)S(1)}) custom-call(bf16[48,2048]{1,0:T(8,128)(2,1)S(1)} %collective-permute-done.refs_0_, bf16[48,2048]{1,0:T(8,128)(2,1)S(1)} %collective-permute-done.1.refs_1_, bf16[2048,512]{1,0:T(8,128)(2,1)S(1)} %copy-done, ...), custom_call_target="tpu_custom_call" | custom-call | flops 402653184 | bytes 4784128 | tf_op jit(solution)/shard_map/pallas_call | solution.py:193
  32.8 1.8 %collective-permute-start.7 = (f32[1,24,128]{2,1,0:T(8,128)S(1)}, f32[1,24,128]{2,1,0:T(8,128)S(1)}, u32[]{:S(2)}, u32[]{:S(2)}) collective-permute-start(f32[1,24,128]{2,1,0:T(8,128)S(1)} %bitcast.9), channel_id=1, source_target_pairs={{0,4},{4,0},{8,12},{12,8},{1,5},{5,1},{9,13},{13,9},{2,6},{6,2},{1... | collective-permute-start | bytes 36872 | tf_op jit(solution)/shard_map/ppermute | solution.py:304
  34.6 2.6 %collective-permute-start.8 = (f32[1,24,128]{2,1,0:T(8,128)S(1)}, f32[1,24,128]{2,1,0:T(8,128)S(1)}, u32[]{:S(2)}, u32[]{:S(2)}) collective-permute-start(f32[1,24,128]{2,1,0:T(8,128)S(1)} %bitcast.10), channel_id=1, source_target_pairs={{0,8},{4,12},{8,0},{12,4},{1,9},{5,13},{9,1},{13,5},{2,10},{6,14},... | collective-permute-start | bytes 36872 | tf_op jit(solution)/shard_map/ppermute | solution.py:304
  37.2 2.0 %collective-permute-done.8.refs_2_ = f32[1,24,128]{2,1,0:T(8,128)S(1)} collective-permute-done((f32[1,24,128]{2,1,0:T(8,128)S(1)}, f32[1,24,128]{2,1,0:T(8,128)S(1)}, u32[]{:S(2)}, u32[]{:S(2)}) %collective-permute-start.8) | collective-permute-done | bytes 12320 | tf_op jit(solution)/shard_map/ppermute | solution.py:304
  39.2 3.5 %collective-permute-done.9.refs_3_ = f32[1,24,128]{2,1,0:T(8,128)S(1)} collective-permute-done((f32[1,24,128]{2,1,0:T(8,128)S(1)}, f32[1,24,128]{2,1,0:T(8,128)S(1)}, u32[]{:S(2)}, u32[]{:S(2)}) %collective-permute-start.9) | collective-permute-done | bytes 12320 | tf_op jit(solution)/shard_map/ppermute | solution.py:304
  42.8 0.5 finish.1
  43.4 1.6 %collective-permute-start.11 = (bf16[1,512]{1,0:T(2,128)(2,1)S(1)}, bf16[1,512]{1,0:T(2,128)(2,1)S(1)}, u32[]{:S(2)}, u32[]{:S(2)}) collective-permute-start(bf16[1,512]{1,0:T(2,128)(2,1)S(1)} %get-tuple-element.41), channel_id=1, source_target_pairs={{0,2},{1,3},{2,0},{3,1},{4,6},{5,7},{6,4},{7,5},{8,10},{9,11},{10,... | collective-permute-start | bytes 3080 | tf_op jit(solution)/shard_map/ppermute | solution.py:304
  45.2 0.7 %store.1 = (bf16[768,512]{1,0:T(8,128)(2,1)}, bf16[768,512]{1,0:T(8,128)(2,1)}) custom-call(bf16[96,512]{1,0:T(8,128)(2,1)S(1)} %get-tuple-element.32.k_rows, bf16[96,512]{1,0:T(8,128)(2,1)S(1)} %get-tuple-element.33.v_rows, bf16[768,512]{1,0:T(8,128)(2,1)} %get-tuple-element.34.k_in, ...), custom_call_target="tpu_custom_call", output_to_operand_aliasing={{0}: (2, {}), {1}: (3, {})} | custom-call | tf_op jit(solution)/shard_map/store/pallas_call | solution.py:219
  45.9 1.1 %collective-permute-done.11 = bf16[1,512]{1,0:T(2,128)(2,1)S(1)} collective-permute-done((bf16[1,512]{1,0:T(2,128)(2,1)S(1)}, bf16[1,512]{1,0:T(2,128)(2,1)S(1)}, u32[]{:S(2)}, u32[]{:S(2)}) %collective-permute-start.11) | collective-permute-done | bytes 1056 | tf_op jit(solution)/shard_map/ppermute | solution.py:304
  47.0 0.9 %collective-permute-done.12 = bf16[1,512]{1,0:T(2,128)(2,1)S(1)} collective-permute-done((bf16[1,512]{1,0:T(2,128)(2,1)S(1)}, bf16[1,512]{1,0:T(2,128)(2,1)S(1)}, u32[]{:S(2)}, u32[]{:S(2)}) %collective-permute-start.12) | collective-permute-done | bytes 1056 | tf_op jit(solution)/shard_map/ppermute | solution.py:304
  47.9 0.6 %add_convert_fusion.1 = bf16[1,512]{1,0:T(2,128)(2,1)} fusion(bf16[1,512]{1,0:T(2,128)(2,1)S(1)} %collective-permute-done.12, bf16[1,512]{1,0:T(2,128)(2,1)S(1)} %collective-permute-done.11, bf16[1,512]{1,0:T(2,128)(2,1)S(1)} %collective-permute-done.10, bf16[1,512]{1,0:T(2,128)(2,1)S(1)} %get-tuple-element.39), kind=kLoop, calls=%fused_computation.5 | loop fusion | flops 4096 | bytes 5120 | tf_op jit(solution)/shard_map/convert_element_type | solution.py:374
  (30 shorter events, 0.7 us)
Async XLA Ops:
  0.6 22.9 %copy-start = (bf16[2048,512]{1,0:T(8,128)(2,1)S(1)}, bf16[2048,512]{1,0:T(8,128)(2,1)}, u32[]{:S(2)}) copy-start(bf16[2048,512]{1,0:T(8,128)(2,1)} %refs_2_.7) | copy-start | bytes 6291460
  0.6 22.9 %copy-start.4 = (bf16[1,512]{1,0:T(2,128)(2,1)S(1)}, bf16[1,512]{1,0:T(2,128)(2,1)}, u32[]{:S(2)}) copy-start(bf16[1,512]{1,0:T(2,128)(2,1)} %refs_4_.7) | copy-start | bytes 3076
  2.7 14.6 %collective-permute-start.2 = (bf16[112,2048]{1,0:T(8,128)(2,1)}, bf16[112,2048]{1,0:T(8,128)(2,1)S(1)}, u32[]{:S(2)}, u32[]{:S(2)}) collective-permute-start(bf16[112,2048]{1,0:T(8,128)(2,1)} %get-tuple-element.24), channel_id=1, source_target_pairs={{0,2},{1,3},{2,0},{3,1},{4,6},{5,7},{6,4},{7,5},{8,10},{9,11},{10,... | collective-permute-start | bytes 1376264 | tf_op jit(solution)/shard_map/ppermute | solution.py:304
  5.7 17.8 %collective-permute-start.6 = (bf16[192,2048]{1,0:T(8,128)(2,1)}, bf16[192,2048]{1,0:T(8,128)(2,1)S(1)}, u32[]{:S(2)}, u32[]{:S(2)}) collective-permute-start(bf16[192,2048]{1,0:T(8,128)(2,1)} %bitcast.6), channel_id=1, source_target_pairs={{0,1},{1,0},{2,3},{3,2},{4,5},{5,4},{6,7},{7,6},{8,9},{9,8},{10,11... | collective-permute-start | bytes 2359304 | tf_op jit(solution)/shard_map/ppermute | solution.py:304
  7.3 12.9 %collective-permute-start.4 = (bf16[32,2048]{1,0:T(8,128)(2,1)}, bf16[32,2048]{1,0:T(8,128)(2,1)}, u32[]{:S(2)}, u32[]{:S(2)}) collective-permute-start(bf16[32,2048]{1,0:T(8,128)(2,1)} %shard_map.95), channel_id=1, source_target_pairs={{0,2},{1,3},{2,0},{3,1},{4,6},{5,7},{6,4},{7,5},{8,10},{9,11},{10,... | collective-permute-start | bytes 393224 | tf_op jit(solution)/shard_map/ppermute | solution.py:304
  7.5 16.0 %collective-permute-start = (bf16[48,2048]{1,0:T(8,128)(2,1)}, bf16[48,2048]{1,0:T(8,128)(2,1)S(1)}, u32[]{:S(2)}, u32[]{:S(2)}) collective-permute-start(bf16[48,2048]{1,0:T(8,128)(2,1)} %get-tuple-element.23), channel_id=1, source_target_pairs={{0,2},{1,3},{2,0},{3,1},{4,6},{5,7},{6,4},{7,5},{8,10},{9,11},{10,... | collective-permute-start | bytes 589832 | tf_op jit(solution)/shard_map/ppermute | solution.py:304
  9.4 14.1 %copy-start.1 = (bf16[2048,512]{1,0:T(8,128)(2,1)S(1)}, bf16[2048,512]{1,0:T(8,128)(2,1)}, u32[]{:S(2)}) copy-start(bf16[2048,512]{1,0:T(8,128)(2,1)} %refs_3_.7) | copy-start | bytes 6291460
  17.3 12.4 %collective-permute-start.3 = (bf16[112,2048]{1,0:T(8,128)(2,1)S(1)}, bf16[112,2048]{1,0:T(8,128)(2,1)S(1)}, u32[]{:S(2)}, u32[]{:S(2)}) collective-permute-start(bf16[112,2048]{1,0:T(8,128)(2,1)S(1)} %collective-permute-done.2.refs_0_), channel_id=1, source_target_pairs={{0,1},{1,0},{2,3},{3,2},{4,5},{5,4},{6,7},{7,6},{8,9},{9,8},{10,11... | collective-permute-start | bytes 1376264 | tf_op jit(solution)/shard_map/ppermute | solution.py:304
  20.2 7.0 %collective-permute-start.5 = (bf16[32,2048]{1,0:T(8,128)(2,1)}, bf16[32,2048]{1,0:T(8,128)(2,1)S(1)}, u32[]{:S(2)}, u32[]{:S(2)}) collective-permute-start(bf16[32,2048]{1,0:T(8,128)(2,1)} %collective-permute-done.4.refs_0_), channel_id=1, source_target_pairs={{0,1},{1,0},{2,3},{3,2},{4,5},{5,4},{6,7},{7,6},{8,9},{9,8},{10,11... | collective-permute-start | bytes 393224 | tf_op jit(solution)/shard_map/ppermute | solution.py:304
  23.5 8.1 %collective-permute-start.1 = (bf16[48,2048]{1,0:T(8,128)(2,1)S(1)}, bf16[48,2048]{1,0:T(8,128)(2,1)S(1)}, u32[]{:S(2)}, u32[]{:S(2)}) collective-permute-start(bf16[48,2048]{1,0:T(8,128)(2,1)S(1)} %collective-permute-done.refs_0_), channel_id=1, source_target_pairs={{0,1},{1,0},{2,3},{3,2},{4,5},{5,4},{6,7},{7,6},{8,9},{9,8},{10,11... | collective-permute-start | bytes 589832 | tf_op jit(solution)/shard_map/ppermute | solution.py:304
  23.5 1.1 %copy-start.2 = (bf16[1,192,2048]{2,1,0:T(8,128)(2,1)S(1)}, bf16[1,192,2048]{2,1,0:T(8,128)(2,1)}, u32[]{:S(2)}) copy-start(bf16[1,192,2048]{2,1,0:T(8,128)(2,1)} %param.7) | copy-start | bytes 2359300
  31.6 11.1 %copy-start.6 = (f32[4]{0:T(128)S(1)}, f32[4]{0:T(128)}, u32[]{:S(2)}) copy-start(f32[4]{0:T(128)} %param.11) | copy-start | bytes 52
  31.6 11.2 %copy-start.3 = (bf16[512,2048]{1,0:T(8,128)(2,1)S(1)}, bf16[512,2048]{1,0:T(8,128)(2,1)}, u32[]{:S(2)}) copy-start(bf16[512,2048]{1,0:T(8,128)(2,1)} %refs_6_.1) | copy-start | bytes 6291460
  31.6 11.2 %copy-start.5 = (f32[128]{0:T(128)S(1)}, f32[128]{0:T(128)}, u32[]{:S(2)}) copy-start(f32[128]{0:T(128)} %param.12) | copy-start | bytes 1540
  32.8 4.4 %collective-permute-start.7 = (f32[1,24,128]{2,1,0:T(8,128)S(1)}, f32[1,24,128]{2,1,0:T(8,128)S(1)}, u32[]{:S(2)}, u32[]{:S(2)}) collective-permute-start(f32[1,24,128]{2,1,0:T(8,128)S(1)} %bitcast.9), channel_id=1, source_target_pairs={{0,4},{4,0},{8,12},{12,8},{1,5},{5,1},{9,13},{13,9},{2,6},{6,2},{1... | collective-permute-start | bytes 36872 | tf_op jit(solution)/shard_map/ppermute | solution.py:304
  34.6 4.6 %collective-permute-start.8 = (f32[1,24,128]{2,1,0:T(8,128)S(1)}, f32[1,24,128]{2,1,0:T(8,128)S(1)}, u32[]{:S(2)}, u32[]{:S(2)}) collective-permute-start(f32[1,24,128]{2,1,0:T(8,128)S(1)} %bitcast.10), channel_id=1, source_target_pairs={{0,8},{4,12},{8,0},{12,4},{1,9},{5,13},{9,1},{13,5},{2,10},{6,14},... | collective-permute-start | bytes 36872 | tf_op jit(solution)/shard_map/ppermute | solution.py:304
  37.2 5.5 %collective-permute-start.9 = (f32[1,24,128]{2,1,0:T(8,128)S(1)}, f32[1,24,128]{2,1,0:T(8,128)S(1)}, u32[]{:S(2)}, u32[]{:S(2)}) collective-permute-start(f32[1,24,128]{2,1,0:T(8,128)S(1)} %bitcast.11), channel_id=1, source_target_pairs={{0,12},{4,8},{8,4},{12,0},{1,13},{5,9},{9,5},{13,1},{2,14},{6,10},... | collective-permute-start | bytes 36872 | tf_op jit(solution)/shard_map/ppermute | solution.py:304
  43.3 2.6 %collective-permute-start.10 = (bf16[1,512]{1,0:T(2,128)(2,1)S(1)}, bf16[1,512]{1,0:T(2,128)(2,1)S(1)}, u32[]{:S(2)}, u32[]{:S(2)}) collective-permute-start(bf16[1,512]{1,0:T(2,128)(2,1)S(1)} %get-tuple-element.40), channel_id=1, source_target_pairs={{0,1},{1,0},{2,3},{3,2},{4,5},{5,4},{6,7},{7,6},{8,9},{9,8},{10,11... | collective-permute-start | bytes 3080 | tf_op jit(solution)/shard_map/ppermute | solution.py:304
  43.4 3.7 %collective-permute-start.11 = (bf16[1,512]{1,0:T(2,128)(2,1)S(1)}, bf16[1,512]{1,0:T(2,128)(2,1)S(1)}, u32[]{:S(2)}, u32[]{:S(2)}) collective-permute-start(bf16[1,512]{1,0:T(2,128)(2,1)S(1)} %get-tuple-element.41), channel_id=1, source_target_pairs={{0,2},{1,3},{2,0},{3,1},{4,6},{5,7},{6,4},{7,5},{8,10},{9,11},{10,... | collective-permute-start | bytes 3080 | tf_op jit(solution)/shard_map/ppermute | solution.py:304
  44.9 3.0 %collective-permute-start.12 = (bf16[1,512]{1,0:T(2,128)(2,1)S(1)}, bf16[1,512]{1,0:T(2,128)(2,1)S(1)}, u32[]{:S(2)}, u32[]{:S(2)}) collective-permute-start(bf16[1,512]{1,0:T(2,128)(2,1)S(1)} %get-tuple-element.42), channel_id=1, source_target_pairs={{0,3},{1,2},{2,1},{3,0},{4,7},{5,6},{6,5},{7,4},{8,11},{9,10},{10,... | collective-permute-start | bytes 3080 | tf_op jit(solution)/shard_map/ppermute | solution.py:304
